TPU v7x, 512 devices: a whole 4x4x16 slice. The times are simulated.
512 devices in a mesh: ep: 32 (over z, core), tp: 16 (over y, x).
Axes of the slice: x: 4, y: 4, z: 16, core: 2. Of those that a mesh axis runs over, the one named last changes fastest.
Arguments:
- tokens: bfloat16 [65536, 2048], P(('ep', 'tp')), may hold values from -6 to 6
- norm_gain: float32 [2048], replicated, may hold values from 0.1 to 1.9
- expert_ids: int32 [65536, 2], P(('ep', 'tp')), may hold values from 0 to 31, all different within a row; in each aligned block of 128 rows (0 to 127, 128 to 255, ...) at most 16 rows name the same one
- gate_weights: float32 [65536, 2], P(('ep', 'tp')), may hold values from 0.2 to 1.6
- expert_gate: bfloat16 [32, 512, 2048], P('ep', 'tp'), may hold values from -0.125 to 0.125
- expert_up: bfloat16 [32, 512, 2048], P('ep', 'tp'), may hold values from -0.125 to 0.125
- expert_down: bfloat16 [32, 512, 2048], P('ep', 'tp'), may hold values from -0.25 to 0.25
- shared_gate: bfloat16 [512, 2048], P('tp'), may hold values from -0.125 to 0.125
- shared_up: bfloat16 [512, 2048], P('tp'), may hold values from -0.125 to 0.125
- shared_down: bfloat16 [512, 2048], P('tp'), may hold values from -0.25 to 0.25
Outputs:
- mixed: bfloat16 [65536, 2048], P(('ep', 'tp'))
Inputs may be any that keep to these rules, and one draw needn't show every extreme that they name: `expert_ids`: each row names 2 different experts. Within the rows of one device no expert is named by more than 16 rows, and in every draw some expert is named by exactly 16 rows of some device.
All inputs are finite; a program needn't handle non-finite values.
Results may differ from a plain program's by a relative error of at most 0.0068.
Values may be sent and summed in bfloat16 or wider, within the bound.
A program may use at most 64 MiB of HBM per device.

v0:
```python
import functools

import jax
import jax.numpy as jnp
from jax import lax
from jax.experimental import pallas as pl
from jax.experimental.pallas import tpu as pltpu
from jax.sharding import PartitionSpec as P

EPS = 1e-06
MESH = pl.DeviceIdType.MESH
BF = jnp.bfloat16
F32 = jnp.float32
NX = 4
NZ = 16
TOK = 128
D = 2048
CAP = 16
NE = 32
COLS = 512
ND = D // COLS
NT = (((1,), (1,)), ((), ()))
STEPS = (0, 1, 2, 1)
ORDER = sorted(range(NX * NX), key=lambda i: (i // NX > 0, STEPS[i % NX] + STEPS[i // NX]))


def kernel(
    tokens, gain_in, ids_in, gw_in, eg, eu, ed, shg, shu, shd, out,
    tok, gain, ids, gw, xt, meta, sw, shid, part, pin, own, placed, rows, act, hid, wgu, wd, res, ret, wt,
    zrecv, zsend, gsend, loc, xrecv, mrecv, srecv, crecv, prow, pinr, retr, sends, credit,
):
    ep, p = lax.axis_index("ep"), lax.axis_index("tp")
    z, c = ep // 2, ep % 2
    x, y = p % NX, p // NX
    delta = (z - (p + 8 * c) + 2 * NZ) % NZ
    far = jnp.minimum(delta, NZ - delta)
    go_up = delta <= 7
    go_down = (delta == 0) | (delta >= 10)
    ep_up = ((z + 1) % NZ) * 2 + c
    ep_down = ((z + NZ - 1) % NZ) * 2 + c
    target = (z + 8 * c) % NZ
    here = p == target
    relative = ((y - target // NX + NX) % NX) * NX + (x - target % NX + NX) % NX
    rank = jnp.int32(0)
    for i, where in enumerate(ORDER):
        rank = jnp.where(relative == where, i, rank)

    def arrived(ref, sem):
        pltpu.make_async_copy(ref, ref, sem).wait()

    def send(src, dst, ssem, rsem, device):
        pltpu.make_async_remote_copy(
            src_ref=src, dst_ref=dst, send_sem=ssem, recv_sem=rsem,
            device_id=device, device_id_type=MESH,
        ).start()

    pltpu.make_async_copy(tokens, tok, loc.at[0]).start()
    pltpu.make_async_copy(ids_in, ids, loc.at[1]).start()
    pltpu.make_async_copy(gain_in, gain, loc.at[2]).start()
    pltpu.make_async_copy(gw_in, gw, loc.at[3]).start()

    barrier = pltpu.get_barrier_semaphore()

    def greet(i, carry):
        @pl.when(jnp.logical_or(i // 2 != p, i % 2 != c))
        def _():
            pl.semaphore_signal(barrier, inc=1, device_id=(z * 2 + i % 2, i // 2), device_id_type=MESH)
        return carry

    with jax.named_scope("greet"):
        lax.fori_loop(0, NE, greet, 0)
        pl.semaphore_signal(barrier, inc=1, device_id=(ep_up, p), device_id_type=MESH)
        pl.semaphore_signal(barrier, inc=1, device_id=(ep_down, p), device_id_type=MESH)

    early, late = [], []
    for m, ref in enumerate((eg, eu)):
        for h in range(2):
            early.append((ref.at[h], wgu.at[m, rank, h], rank * 4 + m * 2 + h))
    for n in range(ND):
        cols = pl.ds(n * COLS, COLS)
        late.append((ed.at[:, cols], wd.at[rank, :, cols], 64 + n * 16 + rank))

    @pl.when(here)
    def _():
        for src, dst, k in early + late:
            pltpu.make_async_copy(src, dst, zrecv.at[k]).start()

    for m, ref in enumerate((shg, shu, shd)):
        pltpu.make_async_copy(ref, sw.at[m, y], srecv.at[y]).start()

    pltpu.make_async_copy(ids_in, ids, loc.at[1]).wait()
    ids0, ids1 = ids[0:1, :], ids[1:2, :]
    e_iota = lax.broadcasted_iota(jnp.int32, (NE, TOK), 0)
    h0 = e_iota == ids0
    h1 = e_iota == ids1
    one, zero = jnp.float32(1), jnp.float32(0)
    hits = (jnp.where(h0, one, zero) + jnp.where(h1, one, zero)).astype(BF)
    earlier = jnp.where(
        lax.broadcasted_iota(jnp.int32, (TOK, TOK), 0) < lax.broadcasted_iota(jnp.int32, (TOK, TOK), 1), one, zero
    ).astype(BF)
    before = jnp.dot(hits, earlier, preferred_element_type=F32)
    slot0 = jnp.sum(jnp.where(h0, before, zero), axis=0, keepdims=True)
    slot1 = jnp.sum(jnp.where(h1, before, zero), axis=0, keepdims=True)
    pos0 = ids0.astype(F32) * CAP + slot0
    pos1 = ids1.astype(F32) * CAP + slot1
    sub = lax.broadcasted_iota(jnp.int32, (8, TOK), 0)
    meta[x] = jnp.where(sub == 0, jnp.broadcast_to(pos0, (8, TOK)), jnp.broadcast_to(pos1, (8, TOK)))

    pltpu.make_async_copy(gain_in, gain, loc.at[2]).wait()
    pltpu.make_async_copy(tokens, tok, loc.at[0]).wait()
    g = gain[...]

    def norm(i, carry):
        at = pl.ds(pl.multiple_of(i * 16, 16), 16)
        t = tok[at, :].astype(F32)
        scale = lax.rsqrt(jnp.mean(t * t, axis=-1, keepdims=True) + EPS)
        xt[x, at, :] = (t * scale * g).astype(BF)
        return carry

    with jax.named_scope("norm"):
        lax.fori_loop(0, TOK // 16, norm, 0)

    with jax.named_scope("meet"):
        pl.semaphore_wait(barrier, NE + 1)

    def gather(pieces, sem):
        @pl.when(jnp.logical_not(here))
        def _():
            for src, dst, k in pieces:
                send(src, dst, sem, zrecv.at[k], (ep, target))

    def turn(first, last):
        if first > 1:
            @pl.when(here)
            def _():
                for i in range(first, last + 1):
                    dx, dy = ORDER[i] % NX, ORDER[i] // NX
                    pl.semaphore_signal(
                        credit, inc=1, device_id=(ep, (y + dy) % NX * NX + (x + dx) % NX), device_id_type=MESH
                    )

        @pl.when(jnp.logical_and(rank >= first, rank <= last))
        def _():
            if first > 1:
                with jax.named_scope("credit"):
                    pl.semaphore_wait(credit, 1)
            for src, dst, k in early:
                send(src, dst, gsend.at[0], zrecv.at[k], (ep, target))

    turn(1, 4)

    def share_tokens():
        for i in (1, 3, 2):
            peer = (ep, y * NX + (x + i) % NX)
            send(meta.at[x], meta.at[x], sends.at[0], mrecv.at[x], peer)
            send(xt.at[x], xt.at[x], sends.at[1], xrecv.at[x], peer)

    def pass_on(ref, k, which):
        arrived(ref, zrecv.at[k])

        @pl.when(go_up)
        def _():
            send(ref, ref, zsend.at[which], zrecv.at[k], (ep_up, p))

        @pl.when(go_down)
        def _():
            send(ref, ref, zsend.at[2 + which], zrecv.at[k], (ep_down, p))

    def gu_step(i, carry):
        pass_on(wgu.at[(i // 2) % 2, i // 4, i % 2], i, 0)
        return carry

    def d_step(i, carry):
        n, s = (i - 64) // 16, i % 16
        pass_on(wd.at[s, :, pl.ds(pl.multiple_of(n * COLS, COLS), COLS)], i, 1)
        return carry

    done = [0]

    def stream(time=None, least=0, more=0):
        a = done[0]
        b = jnp.minimum(a + jnp.where(go_up | go_down, more, 0), 128)
        b = jnp.maximum(b, least)
        if time is not None:
            left = time - 10 - (34 - 6 * c) * far
            k = jnp.where(left < 451, jnp.maximum(left, 0) * 10 // 71, 64 + (left - 451) * 10 // 36)
            b = jnp.maximum(b, jnp.minimum(k, 128))
        with jax.named_scope("s"):
            lax.fori_loop(jnp.minimum(a, 64), jnp.minimum(b, 64), gu_step, 0)
            lax.fori_loop(jnp.maximum(a, 64), jnp.maximum(b, 64), d_step, 0)
        done[0] = b

    def weigh():
        pltpu.make_async_copy(gw_in, gw, loc.at[3]).wait()
        slot_iota = lax.broadcasted_iota(jnp.int32, (NE * CAP, TOK), 0).astype(F32)
        w = jnp.where(slot_iota == pos0, gw[0:1, :], zero) + jnp.where(slot_iota == pos1, gw[1:2, :], zero)
        w = w.T
        w_hi = w.astype(BF)
        wt[0] = w_hi
        wt[1] = (w - w_hi.astype(F32)).astype(BF)

    def place(i):
        with jax.named_scope(f"place{i}"):
            s = (x + i) % NX
            if i:
                arrived(meta.at[s], mrecv.at[s])
                arrived(xt.at[s], xrecv.at[s])
            row = lax.broadcasted_iota(jnp.int32, (TOK, TOK), 0)
            dest, slot = row >> 4, row & 15
            dy, dc = dest >> 1, dest & 1
            expert = 2 * ((4 * dy + x + 8 * dc) & 15) + dc
            aim = (expert * CAP + slot).astype(F32)
            m = meta[s]
            onehot = jnp.where((aim == m[0:1, :]) | (aim == m[1:2, :]), one, zero).astype(BF)
            for j in range(ND):
                cols = pl.ds(j * COLS, COLS)
                placed[s, :, :, cols] = (
                    jnp.dot(onehot, xt[s, :, cols], preferred_element_type=F32).astype(BF).reshape(8, CAP, COLS)
                )
            src = (y * 2 + c) * NX + s
            rows[src] = placed[s, y * 2 + c]
            for q in range(1, 8):
                dest = (y * 2 + c + q) % 8
                send(placed.at[s, dest], rows.at[src], sends.at[3], prow, (z * 2 + dest % 2, (dest // 2) * NX + x))

    def share_weights():
        for i in (1, 3, 2):
            peer = (ep, ((y + i) % NX) * NX + x)
            for m, ref in enumerate((shg, shu, shd)):
                send(ref.at[c], sw.at[m, y, c], sends.at[2], srecv.at[y], peer)

    def cross():
        with jax.named_scope("cross"):
            for i in (1, 3, 2):
                s = (y + i) % NX
                arrived(sw.at[:, s, c], srecv.at[s])
                send(sw.at[:, s, c], sw.at[:, s, c], sends.at[6], crecv.at[s], (z * 2 + 1 - c, p))

    def shared_up(i):
        with jax.named_scope("sharedu"):
            s = (x + i) % NX
            if i == 0:
                arrived(sw.at[:, y], srecv.at[y])
                for q in range(1, NX):
                    arrived(sw.at[:, (y + q) % NX, 1 - c], crecv.at[(y + q) % NX])
            blk = xt[s]
            a = lax.dot_general(blk, sw[0].reshape(TOK, D), NT, preferred_element_type=F32)
            b = lax.dot_general(blk, sw[1].reshape(TOK, D), NT, preferred_element_type=F32)
            shid[...] = (a / (1.0 + jnp.exp(-a)) * b).astype(BF)

    def shared_down(i):
        with jax.named_scope("sharedd"):
            s = (x + i) % NX
            down = sw.at[2]
            for j in range(ND):
                cols = pl.ds(j * COLS, COLS)
                v = jnp.dot(shid[...], down[:, :, :, cols].reshape(TOK, COLS), preferred_element_type=F32)
                if i == 0:
                    own[:, cols] = v
                else:
                    part[s, :, cols] = v.astype(BF)
            if i:
                send(part.at[s], pin.at[x], sends.at[4], pinr.at[x], (ep, y * NX + s))

    HALF = NE * CAP // 2

    def hidden(r, b, m):
        with jax.named_scope("hidden"):
            blk = rows[16 * b:16 * b + 16].reshape(HALF, D)
            v = lax.dot_general(blk, wgu[m, 8 * r:8 * r + 8].reshape(256, D), NT, preferred_element_type=F32)
            if m == 0:
                act[...] = v / (1.0 + jnp.exp(-v))
            else:
                hid[r, b * HALF:(b + 1) * HALF, :] = (act[...] * v).astype(BF)

    me = 2 * ((p + 8 * c) % NZ) + c
    me_src = (y * 2 + c) * NX + x

    def result(n):
        with jax.named_scope("result"):
            cols = pl.ds(n * COLS, COLS)
            for b in range(2):
                at = pl.ds(b * HALF, HALF)
                v = jnp.dot(hid[0, at, :], wd[0:8, :, cols].reshape(256, COLS), preferred_element_type=F32)
                v = v + jnp.dot(hid[1, at, :], wd[8:16, :, cols].reshape(256, COLS), preferred_element_type=F32)
                res[16 * b:16 * b + 16, :, cols] = v.astype(BF).reshape(16, CAP, COLS)
            ret[me, :, cols] = res[me_src, :, cols]

    def give_back(n, a, b):
        cols = pl.ds(n * COLS, COLS)

        def one_block(i, carry):
            q = (me_src + i) % NE
            qy, qc, qx = q // 8, (q // 4) % 2, q % 4
            send(res.at[q, :, cols], ret.at[me, :, cols], sends.at[5], retr.at[n], (z * 2 + qc, qy * NX + qx))
            return carry

        with jax.named_scope("give"):
            lax.fori_loop(a, b, one_block, 0)

    def take_part(i):
        s = (x + i) % NX
        with jax.named_scope("pin"):
            arrived(pin.at[s], pinr.at[s])
            for j in range(ND):
                cols = pl.ds(j * COLS, COLS)
                own[:, cols] = own[:, cols] + pin[s, :, cols].astype(F32)

    weigh()
    stream(time=50)
    turn(5, 8)
    stream(time=110)
    turn(9, 12)
    stream(time=130)

    @pl.when(far > 3)
    def _():
        pl.delay(11000)

    share_tokens()
    place(0)
    stream(time=170)
    turn(13, 15)
    share_weights()
    stream(time=280)
    gather(late, gsend.at[1])
    stream(time=455)
    place(1)
    stream(time=460)
    place(3)
    stream(time=475)
    place(2)
    stream(time=510)
    cross()
    stream(time=560)
    for i in (0, 1, 3, 2):
        shared_up(i)
        stream(more=2)
        shared_down(i)
        stream(more=2)
    stream(time=690, least=32)
    with jax.named_scope("wait_rows"):
        arrived(rows.at[pl.ds(0, 28)], prow)
    stream(least=64)
    for r in range(2):
        for b in range(2):
            for m in range(2):
                hidden(r, b, m)
                stream(more=3)
    for n in range(ND):
        stream(least=64 + 16 * n + 16)
        result(n)
        stream(more=3)
        give_back(n, 1, 16)
        stream(more=3)
        give_back(n, 16, NE)
        stream(more=3)
    for i in (1, 3, 2):
        take_part(i)

    for n in range(ND):
        cols = pl.ds(n * COLS, COLS)
        with jax.named_scope(f"wait_ret{n}"):
            arrived(ret.at[pl.ds(0, NE - 1), :, cols], retr.at[n])
        with jax.named_scope("combine"):
            blk = ret[:, :, cols].reshape(NE * CAP, COLS)
            v = jnp.dot(wt[0], blk, preferred_element_type=F32) + jnp.dot(wt[1], blk, preferred_element_type=F32)
            out[:, cols] = (v + own[:, cols]).astype(BF)

    @pl.when(jnp.logical_not(here))
    def _():
        arrived(wgu.at[0, pl.ds(0, 2)], gsend.at[0])
        arrived(wd.at[0], gsend.at[1])

    @pl.when(go_up)
    def _():
        arrived(wgu, zsend.at[0])
        arrived(wd, zsend.at[1])

    @pl.when(go_down)
    def _():
        arrived(wgu, zsend.at[2])
        arrived(wd, zsend.at[3])

    arrived(meta.at[pl.ds(0, 3)], sends.at[0])
    arrived(xt.at[pl.ds(0, 3)], sends.at[1])
    arrived(sw.at[:, pl.ds(0, 3), 0], sends.at[2])
    arrived(sw.at[:, pl.ds(0, 3), 0], sends.at[6])
    arrived(rows.at[pl.ds(0, 28)], sends.at[3])
    arrived(pin.at[pl.ds(0, 3)], sends.at[4])
    arrived(ret.at[pl.ds(0, NE - 1)], sends.at[5])


def body(tokens, norm_gain, expert_ids, gate_weights, expert_gate, expert_up, expert_down, shared_gate, shared_up, shared_down):
    anywhere = pl.BlockSpec(memory_space=pl.ANY)
    dma = pltpu.SemaphoreType.DMA
    return pl.pallas_call(
        kernel,
        out_shape=jax.ShapeDtypeStruct((TOK, D), BF),
        in_specs=[anywhere] * 10,
        out_specs=pl.BlockSpec(memory_space=pltpu.VMEM),
        scratch_shapes=[
            pltpu.VMEM((TOK, D), BF),
            pltpu.VMEM((1, D), F32),
            pltpu.VMEM((2, TOK), jnp.int32),
            pltpu.VMEM((2, TOK), F32),
            pltpu.VMEM((NX, TOK, D), BF),
            pltpu.VMEM((NX, 8, TOK), F32),
            pltpu.VMEM((3, NX, 2, 16, D), BF),
            pltpu.VMEM((TOK, TOK), BF),
            pltpu.VMEM((NX, TOK, D), BF),
            pltpu.VMEM((NX, TOK, D), BF),
            pltpu.VMEM((TOK, D), F32),
            pltpu.VMEM((NX, 8, CAP, D), BF),
            pltpu.VMEM((NE, CAP, D), BF),
            pltpu.VMEM((NE * CAP // 2, 256), F32),
            pltpu.VMEM((2, NE * CAP, 256), BF),
            pltpu.VMEM((2, 16, 2, 16, D), BF),
            pltpu.VMEM((16, 32, D), BF),
            pltpu.VMEM((NE, CAP, D), BF),
            pltpu.VMEM((NE, CAP, D), BF),
            pltpu.VMEM((2, TOK, NE * CAP), BF),
            dma((128,)),
            dma((4,)),
            dma((2,)),
            dma((4,)),
            dma((NX,)),
            dma((NX,)),
            dma((NX,)),
            dma((NX,)),
            dma,
            dma((NX,)),
            dma((ND,)),
            dma((7,)),
            pltpu.SemaphoreType.REGULAR,
        ],
        compiler_params=pltpu.CompilerParams(
            collective_id=0, has_side_effects=True, vmem_limit_bytes=48000 * 1024
        ),
    )(
        *[pltpu.with_memory_space_constraint(a, pltpu.HBM) for a in (
            tokens,
        norm_gain.reshape(1, D),
        expert_ids.T,
        gate_weights.T,
        expert_gate.reshape(2, 16, D),
        expert_up.reshape(2, 16, D),
        expert_down.reshape(32, D),
        shared_gate.reshape(2, 16, D),
        shared_up.reshape(2, 16, D),
        shared_down.reshape(2, 16, D),
        )]
    )


def solution(mesh):
    in_specs = (
        P(("ep", "tp"), None),
        P(),
        P(("ep", "tp"), None),
        P(("ep", "tp"), None),
        P("ep", "tp", None),
        P("ep", "tp", None),
        P("ep", "tp", None),
        P("tp", None),
        P("tp", None),
        P("tp", None),
    )
    out_specs = P(("ep", "tp"), None)
    return jax.shard_map(body, mesh=mesh, in_specs=in_specs, out_specs=out_specs, check_vma=False)
```

profile of v0, /device:TPU:3, one launch (start us, length us, event | category | flops | bytes accessed | tf_op | source)
XLA Modules:
  0.0 134.0 jit_solution(9632954117798890077)
XLA Ops:
  0.0 133.2 %shard_map.100 = bf16[128,2048]{1,0:T(8,128)(2,1)S(1)} custom-call(bf16[128,2048]{1,0:T(8,128)(2,1)} %tokens.1, f32[1,2048]{1,0:T(1,128)} %bitcast.15, s32[2,128]{1,0:T(2,128)} %bitcast.16, f32[2,128]{1,0:T(2,128)} %bitcast.17, bf16[2,16,2048]{2,1,0:T(8,128)(2,1)} %bitcast.9, bf16[2,16,2048]{2,1,0:T(8,128)(2,1)} %bitcast.10, bf16[32,2048]{1,0:T(8,128)(2,1)} %bitcast.11, ...), custom_call_target="tpu_custom_call" | custom-call | tf_op jit(solution)/shard_map/pallas_call | solution.py:397
  133.2 0.8 copy.12
where the time goes:
time: 134 us
  Pallas kernels  133 us (99%)
    pallas_call x1, Pallas kernels, body(): pl.pallas_call(kernel, out_shape=jax.ShapeDtypeStruct((TOK, D), BF), in_s...  133 us

commit v1 on v0

--- a/solution.py
+++ b/solution.py
@@ -307,9 +307,9 @@
                 own[:, cols] = own[:, cols] + pin[s, :, cols].astype(F32)
 
     weigh()
-    stream(time=50)
+    stream(time=40)
     turn(5, 8)
-    stream(time=110)
+    stream(time=95)
     turn(9, 12)
     stream(time=130)
 
@@ -319,7 +319,7 @@
 
     share_tokens()
     place(0)
-    stream(time=170)
+    stream(time=150)
     turn(13, 15)
     share_weights()
     stream(time=280)

time: 134 us -> 133 us (level)
  no operation moved by 1% of the time
where the time goes in v1:
time: 133 us
  Pallas kernels  132 us (99%)
    pallas_call x1, Pallas kernels, body(): pl.pallas_call(kernel, out_shape=jax.ShapeDtypeStruct((TOK, D), BF), in_s...  132 us

profile of v1, /device:TPU:3, one launch (start us, length us, event | category | flops | bytes accessed | tf_op | source)
XLA Modules:
  0.0 132.9 jit_solution(15934506167780016516)
XLA Ops:
  0.0 132.1 %shard_map.100 = bf16[128,2048]{1,0:T(8,128)(2,1)S(1)} custom-call(bf16[128,2048]{1,0:T(8,128)(2,1)} %tokens.1, f32[1,2048]{1,0:T(1,128)} %bitcast.15, s32[2,128]{1,0:T(2,128)} %bitcast.16, f32[2,128]{1,0:T(2,128)} %bitcast.17, bf16[2,16,2048]{2,1,0:T(8,128)(2,1)} %bitcast.9, bf16[2,16,2048]{2,1,0:T(8,128)(2,1)} %bitcast.10, bf16[32,2048]{1,0:T(8,128)(2,1)} %bitcast.11, ...), custom_call_target="tpu_custom_call" | custom-call | tf_op jit(solution)/shard_map/pallas_call | solution.py:397
  132.1 0.8 copy.12
